TPU v7x, 32 devices: a whole 2x2x4 slice. The times are simulated.
32 devices in a mesh: grp: 1, ep: 32 (over z, y, x, core).
Axes of the slice: x: 2, y: 2, z: 4, core: 2. Of those that a mesh axis runs over, the one named last changes fastest.
Arguments:
- residual_input: bfloat16 [768, 2048], P(('grp', 'ep')), may hold values from -6 to 6
- attention_norm_gain: bfloat16 [2048], replicated, may hold values from 0.099609375 to 1.8984375
- receptance_weight: bfloat16 [2048, 1024], P(None, 'ep'), may hold values from -0.125 to 0.125
- key_weight: bfloat16 [2048, 1024], P(None, 'ep'), may hold values from -0.125 to 0.125
- value_weight: bfloat16 [2048, 1024], P(None, 'ep'), may hold values from -0.125 to 0.125
- decay_weight: bfloat16 [2048, 1024], P(None, 'ep'), may hold values from -0.125 to 0.125
- correction_rate_weight: bfloat16 [2048, 1024], P(None, 'ep'), may hold values from -0.125 to 0.125
- output_gate_weight: bfloat16 [2048, 1024], P(None, 'ep'), may hold values from -0.125 to 0.125
- decay_offset: float32 [1024], replicated, may hold values from -3 to 1
- correction_rate_offset: float32 [1024], replicated, may hold values from -1.5 to 1.5
- self_term_weight: float32 [1024], replicated, may hold values from -2 to 2
- head_read_gain: float32 [1024], replicated, may hold values from 0.1 to 1.9
- previous_state: float32 [768, 16, 4096], P(('grp', 'ep')), may hold values from -4 to 4
- attention_output_weight: bfloat16 [1024, 2048], replicated, may hold values from -0.1875 to 0.1875
- feedforward_norm_gain: bfloat16 [2048], replicated, may hold values from 0.099609375 to 1.8984375
- routes: int32 [768, 4], P('grp'), may hold values from 0 to 31, all different within a row; in each aligned block of 24 rows (0 to 23, 24 to 47, ...) at most 4 rows name the same one
- routing_weight: float32 [768, 4], P('grp'), may hold values from 0.2 to 1
- routed_gate_weight: bfloat16 [32, 2048, 512], P('ep'), may hold values from -0.125 to 0.125
- routed_up_weight: bfloat16 [32, 2048, 512], P('ep'), may hold values from -0.125 to 0.125
- routed_down_weight: bfloat16 [32, 512, 2048], P('ep'), may hold values from -0.25 to 0.25
- common_gate_weight: bfloat16 [2048, 512], replicated, may hold values from -0.125 to 0.125
- common_up_weight: bfloat16 [2048, 512], replicated, may hold values from -0.125 to 0.125
- common_down_weight: bfloat16 [512, 2048], replicated, may hold values from -0.25 to 0.25
Outputs:
- hidden_out: bfloat16 [768, 2048], P(('grp', 'ep'))
- next_state: float32 [768, 16, 4096], P(('grp', 'ep'))
Inputs may be any that keep to these rules, and one draw needn't show every extreme that they name: `routes`: the 4 entries of a row differ. In each aligned block of 24 rows (the tokens of one index of ep) no expert is named by more than 4 rows, a bound that some block reaches.
All inputs are finite; a program needn't handle non-finite values.
Results may differ from a plain program's by a relative error of at most 0.013.
Values may be sent and summed in bfloat16 or wider, within the bound.
A program may use at most 128 MiB of HBM per device.

v0:
```python
import jax
import jax.numpy as jnp
from jax import lax
from jax.sharding import PartitionSpec as P

HEAD_COUNT = 16
HEAD_SIZE = 64
CAP = 4


def rms_norm(value_rows, gain):
    scale = lax.rsqrt(jnp.mean(value_rows * value_rows, axis=-1, keepdims=True) + 1e-06)
    return (value_rows * scale * gain.astype(jnp.float32)).astype(jnp.bfloat16)


def expert_mlp(rows, gate_w, up_w, down_w):
    gate = jnp.dot(rows, gate_w, preferred_element_type=jnp.float32)
    upward = jnp.dot(rows, up_w, preferred_element_type=jnp.float32)
    hidden = (jax.nn.silu(gate) * upward).astype(jnp.bfloat16)
    return jnp.dot(hidden, down_w, preferred_element_type=jnp.float32).astype(jnp.bfloat16)


def attention_mixer(
    receptance_rows,
    key_rows,
    value_rows,
    decay_logit,
    rate_logit,
    gate_logit,
    decay_offset,
    correction_rate_offset,
    self_term_weight,
    head_read_gain,
    head_state,
):
    tally_value = receptance_rows.shape[0]

    def heads(tensor):
        return tensor.astype(jnp.float32).reshape(tally_value, HEAD_COUNT, HEAD_SIZE)

    decay = jnp.exp(
        -jnp.exp(-jax.nn.softplus(-(decay_offset + decay_logit.astype(jnp.float32))) - 0.5)
    )
    rate = jax.nn.sigmoid(correction_rate_offset + rate_logit.astype(jnp.float32))
    key_head = heads(key_rows)
    rate_head = heads(rate)
    receptance_head = heads(receptance_rows)
    head_value = heads(value_rows)
    unit_key = key_head * lax.rsqrt(1.0 + jnp.sum(key_head * key_head, axis=-1, keepdims=True))
    rate_scaled_key = key_head * rate_head
    removal = unit_key * rate_head
    matrix = head_state.reshape(tally_value, HEAD_COUNT, HEAD_SIZE, HEAD_SIZE)
    recalled = jnp.einsum("nhvk,nhk->nhv", matrix, unit_key, precision=lax.Precision.HIGHEST)
    matrix = (
        matrix * heads(decay)[:, :, None, :]
        - recalled[..., None] * removal[:, :, None, :]
        + head_value[..., None] * rate_scaled_key[:, :, None, :]
    )
    read = jnp.einsum("nhvk,nhk->nhv", matrix, receptance_head, precision=lax.Precision.HIGHEST)
    centered = read - jnp.mean(read, axis=-1, keepdims=True)
    variance = jnp.mean(centered * centered, axis=-1, keepdims=True)
    normed_head_read = (
        centered * lax.rsqrt(variance + 0.00064) * head_read_gain.reshape(HEAD_COUNT, HEAD_SIZE)
    )
    self_term = (
        jnp.sum(
            receptance_head * rate_scaled_key * self_term_weight.reshape(HEAD_COUNT, HEAD_SIZE),
            axis=-1,
            keepdims=True,
        )
        * head_value
    )
    normed_mixer_input = (normed_head_read + self_term).reshape(
        tally_value, HEAD_COUNT * HEAD_SIZE
    ) * jax.nn.sigmoid(gate_logit.astype(jnp.float32))
    return (
        normed_mixer_input.astype(jnp.bfloat16),
        matrix.reshape(tally_value, HEAD_COUNT, HEAD_SIZE * HEAD_SIZE),
    )


def slot_table(block_routes, block_weight, expert_ids):
    match = block_routes[..., None] == expert_ids
    hit = jnp.any(match, axis=-2).astype(jnp.int32)
    weight = jnp.sum(jnp.where(match, block_weight[..., None], 0.0), axis=-2)
    rank = jnp.cumsum(hit, axis=-2) - hit
    slots = jnp.arange(CAP, dtype=jnp.int32)
    select = ((hit[..., None] == 1) & (rank[..., None] == slots)).astype(jnp.float32)
    return (select, weight)


def combine_returned(select, weight, returned):
    coefficient = select * weight[..., None]
    return jnp.einsum(
        "nec,ecd->nd", coefficient, returned.astype(jnp.float32), precision=lax.Precision.HIGHEST
    )


def serve_gathered(
    whole, routes, routing_weight, ep_size, tally_value, expert_ids, gate_w, up_w, down_w
):
    block_routes = routes.reshape(ep_size, tally_value, routes.shape[-1])
    block_weight = routing_weight.reshape(ep_size, tally_value, routing_weight.shape[-1])
    select, weight = slot_table(block_routes, block_weight, expert_ids)
    select = select[:, :, 0, :]
    weight = weight[:, :, 0]
    rows = jnp.einsum(
        "snc,snd->scd",
        select.astype(jnp.bfloat16),
        whole.reshape(ep_size, tally_value, whole.shape[-1]),
        preferred_element_type=jnp.float32,
    ).astype(jnp.bfloat16)
    output = expert_mlp(rows.reshape(-1, rows.shape[-1]), gate_w, up_w, down_w).reshape(rows.shape)
    return (output, select, weight)


def per_device(
    residual_input,
    attention_norm_gain,
    receptance_weight,
    key_weight,
    value_weight,
    decay_weight,
    correction_rate_weight,
    output_gate_weight,
    decay_offset,
    correction_rate_offset,
    self_term_weight,
    head_read_gain,
    previous_state,
    attention_output_weight,
    feedforward_norm_gain,
    routes,
    routing_weight,
    routed_gate_weight,
    routed_up_weight,
    routed_down_weight,
    common_gate_weight,
    common_up_weight,
    common_down_weight,
):
    ep_size = lax.axis_size("ep")
    device = lax.axis_index("ep")
    tally_value = residual_input.shape[0]
    normed = rms_norm(residual_input.astype(jnp.float32), attention_norm_gain)
    stacked = jnp.stack(
        (
            receptance_weight,
            key_weight,
            value_weight,
            decay_weight,
            correction_rate_weight,
            output_gate_weight,
        ),
        axis=1,
    )
    local_cols = jnp.einsum(
        "td,drc->trc",
        lax.all_gather(normed, "ep", axis=0, tiled=True),
        stacked,
        preferred_element_type=jnp.float32,
    ).astype(jnp.bfloat16)
    role_rows = lax.all_to_all(local_cols, "ep", split_axis=0, concat_axis=2, tiled=True)
    normed_mixer_input, next_state = attention_mixer(
        role_rows[:, 0],
        role_rows[:, 1],
        role_rows[:, 2],
        role_rows[:, 3],
        role_rows[:, 4],
        role_rows[:, 5],
        decay_offset,
        correction_rate_offset,
        self_term_weight,
        head_read_gain,
        previous_state,
    )
    attended = jnp.dot(
        normed_mixer_input, attention_output_weight, preferred_element_type=jnp.float32
    ).astype(jnp.bfloat16)
    middle = residual_input.astype(jnp.float32) + attended.astype(jnp.float32)
    normed_ffn = rms_norm(middle, feedforward_norm_gain)
    shared = expert_mlp(normed_ffn, common_gate_weight, common_up_weight, common_down_weight)
    expert_count = routed_gate_weight.shape[0] * ep_size
    all_ids = jnp.arange(expert_count, dtype=jnp.int32)
    own_ids = device.reshape(1)
    own_routes = lax.dynamic_slice_in_dim(routes, device * tally_value, tally_value, 0)
    own_weight = lax.dynamic_slice_in_dim(routing_weight, device * tally_value, tally_value, 0)
    whole = lax.all_gather(normed_ffn, "ep", axis=0, tiled=True)
    output, unused_select, unused_weight = serve_gathered(
        whole,
        routes,
        routing_weight,
        ep_size,
        tally_value,
        own_ids,
        routed_gate_weight[0],
        routed_up_weight[0],
        routed_down_weight[0],
    )
    returned = lax.all_to_all(output, "ep", split_axis=0, concat_axis=0, tiled=True)
    select, weight = slot_table(own_routes, own_weight, all_ids)
    routed = combine_returned(select, weight, returned)
    hidden_out = (middle + shared.astype(jnp.float32) + routed).astype(jnp.bfloat16)
    return (hidden_out, next_state)


def solution(mesh):
    return jax.shard_map(
        per_device,
        mesh=mesh,
        in_specs=(
            P(("grp", "ep"), None),
            P(),
            P(None, "ep"),
            P(None, "ep"),
            P(None, "ep"),
            P(None, "ep"),
            P(None, "ep"),
            P(None, "ep"),
            P(),
            P(),
            P(),
            P(),
            P(("grp", "ep"), None, None),
            P(),
            P(),
            P("grp", None),
            P("grp", None),
            P("ep", None, None),
            P("ep", None, None),
            P("ep", None, None),
            P(),
            P(),
            P(),
        ),
        out_specs=(P(("grp", "ep"), None), P(("grp", "ep"), None, None)),
        check_vma=False,
    )
```

profile of v0, /device:TPU:0, one launch (start us, length us, event | category | flops | bytes accessed | tf_op | source)
XLA Modules:
  0.0 249.9 jit_solution(6900193728107449112)
XLA Ops:
  8.1 1.0 fusion.34
  9.1 1.6 fusion.36
  10.7 0.9 bitcast_dynamic-update-slice_fusion.5
  12.6 0.9 bitcast_dynamic-update-slice_fusion.3
  16.3 57.0 %all-gather.3.cloned.1.call-done = bf16[768,2048]{1,0:T(8,128)(2,1)} async-done(((bf16[24,2048]{1,0:T(8,128)(2,1)}), bf16[768,2048]{1,0:T(8,128)(2,1)}) %all-gather.3.cloned.1.call-update) | async-done | bytes 3145744 | tf_op jit(solution)/shard_map/all_gather | solution.py:159
  73.2 3.1 %fusion.72 = f32[768,192]{0,1:S(1)} fusion(bf16[768,2048]{1,0:T(8,128)(2,1)} %all-gather.3.cloned.1.call-done, bf16[2048,192]{0,1:T(8,128)(2,1)S(1)} %bitcast.99), kind=kOutput, calls=%fused_computation.110 | convolution fusion | flops 603979776 | bytes 4521984
  76.4 1.8 copy.38
  78.2 3.4 %reshape.259 = bf16[32,2,2304]{2,1,0:T(2,128)(2,1)} reshape(bf16[768,6,32]{2,1,0:T(8,128)(2,1)} %copy.38) | data formatting | bytes 589824
  81.6 3.3 %all-to-all-start = ((bf16[32,2,2304]{2,1,0:T(2,128)(2,1)}), bf16[32,2,2304]{2,1,0:T(2,128)(2,1)S(1)}, u32[]{:S(2)}, u32[]{:S(2)}) async-start(bf16[32,2,2304]{2,1,0:T(2,128)(2,1)} %reshape.259), calls=%async_computation | async-start | bytes 589824 | tf_op jit(solution)/shard_map/all_to_all | solution.py:163
  85.3 10.8 %reshape.237 = f32[24,16,64,64]{3,2,1,0:T(8,128)} reshape(f32[24,16,4096]{2,1,0:T(8,128)} %param.35) | data formatting | bytes 12582912 | tf_op jit(solution)/shard_map/reshape | solution.py:52
  96.4 2.2 reshape.260
  98.6 2.2 copy.40
  100.8 1.9 all_to_all.19
  102.7 0.9 slice_convert_fusion.2
  105.5 22.8 %fusion.73 = f32[24,16,1,64]{3,2,1,0:T(1,128)S(1)} fusion(f32[24,16,64,1]{2,3,1,0:T(1,128)S(1)} %bitcast.97, f32[24,16,64,64]{3,2,1,0:T(8,128)} %reshape.237), kind=kOutput, calls=%fused_computation.111 | convolution fusion | flops 18874368 | bytes 6488064 | tf_op jit(solution)/shard_map/nhvk,nhk->nhv/dot_general | solution.py:53
  128.3 16.5 %fusion.1 = f32[24,16,1,64]{3,2,1,0:T(1,128)S(1)} fusion(bf16[24,16,64,1]{2,3,1,0:T(2,128)(2,1)S(1)} %copy-done.6, f32[24,16,64,64]{3,2,1,0:T(8,128)S(1)} %copy-done.1, f32[24,16,64]{2,1,0:T(8,128)S(1)} %fusion.41, f32[24,16,64]{2,1,0:T(8,128)S(1)} %get-tuple-element.2, f32[24,16,64]{2,1,0:T(8,128)S(1)} %bitcast.95, f32[24,16,64]{2,1,0:T(8,128)S(1)} %get-tuple-element.4, ...), kind=kOutput, calls=%fused_computation.1 | convolution fusion | flops 26738688 | bytes 6930432 | tf_op jit(solution)/shard_map/nhvk,nhk->nhv/dot_general | solution.py:59
  146.1 3.0 %multiply_reduce_fusion = (f32[24]{0:T(128)S(1)}, f32[24,2048]{1,0:T(8,128)S(1)}) fusion(bf16[1024,2048]{1,0:T(8,128)(2,1)} %param.36, f32[24,1024]{1,0:T(8,128)S(1)} %reshape.239, bf16[24,6,1024]{2,0,1:T(8,128)(2,1)} %all_to_all.19, bf16[24,2048]{1,0:T(8,128)(2,1)S(1)} %copy-done.3), kind=kOutput, calls=%fused_computation.49 | convolution fusion | flops 101105640 | bytes 4636768 | tf_op jit(solution)/shard_map/dot_general | solution.py:177
  153.2 9.3 %broadcast_multiply_fusion = (f32[24,16,64,64]{3,2,1,0:T(8,128)}, f32[24,16,64,64]{3,2,1,0:T(8,128)}) fusion(f32[24,16,64]{2,1,0:T(8,128)S(1)} %get-tuple-element.4, f32[24,16,64]{2,1,0:T(8,128)S(1)} %reshape.246, f32[24,16,64]{2,1,0:T(8,128)S(1)} %get-tuple-element.2, f32[24,16,64]{2,1,0:T(8,128)S(1)} %bitcast.96), kind=kLoop, calls=%fused_computation.6 | loop fusion | flops 3145728 | bytes 12976128 | tf_op jit(solution)/shard_map/mul | solution.py:57
  162.5 10.8 %mul.247 = f32[24,16,4096]{2,1,0:T(8,128)} reshape(f32[24,16,64,64]{3,2,1,0:T(8,128)} %get-tuple-element.14) | data formatting | bytes 12582912 | tf_op jit(solution)/shard_map/mul | solution.py:57
  173.3 10.9 %mul.246 = f32[24,16,4096]{2,1,0:T(8,128)} reshape(f32[24,16,64,64]{3,2,1,0:T(8,128)} %get-tuple-element.15) | data formatting | bytes 12582912 | tf_op jit(solution)/shard_map/mul | solution.py:56
  184.3 5.4 %mul.206 = f32[24,16,64,64]{3,2,1,0:T(8,128)} broadcast(f32[24,16,64]{2,1,0:T(8,128)S(1)} %copy-done.5), dimensions={0,1,3} | broadcast | bytes 6389760 | tf_op jit(solution)/shard_map/mul | solution.py:55
  189.6 10.9 %mul.244 = f32[24,16,4096]{2,1,0:T(8,128)} reshape(f32[24,16,64,64]{3,2,1,0:T(8,128)} %mul.206) | data formatting | bytes 12582912 | tf_op jit(solution)/shard_map/mul | solution.py:55
  200.6 9.7 %all-gather.5.cloned.1.call-done = bf16[768,2048]{1,0:T(8,128)(2,1)} async-done(((bf16[24,2048]{1,0:T(8,128)(2,1)}), bf16[768,2048]{1,0:T(8,128)(2,1)}) %all-gather.5.cloned.1.call-update) | async-done | bytes 3145744 | tf_op jit(solution)/shard_map/all_gather | solution.py:188
  210.3 2.7 %convolution_convert_fusion.1 = bf16[32,4,2048]{2,1,0:T(4,128)(2,1)S(1)} fusion(bf16[32,24,2048]{2,1,0:T(8,128)(2,1)} %bitcast.91, s32[32,24]{1,0:T(8,128)S(1)} %sub.39, pred[32,24]{1,0:T(8,128)(4,1)S(1)} %broadcast_compare_fusion), kind=kOutput, calls=%fused_computation.10 | convolution fusion | flops 12857344 | bytes 3673856 | tf_op jit(solution)/shard_map/snc,snd->scd/dot_general | solution.py:107
  213.1 2.7 %fusion.15 = f32[128,512]{1,0:T(8,128)} fusion(bf16[128,2048]{1,0:T(8,128)(2,1)S(1)} %reshape.241, bf16[1,2048,512]{2,1,0:T(8,128)(2,1)} %param.40), kind=kOutput, calls=%fused_computation.23 | convolution fusion | flops 268435456 | bytes 2883584 | tf_op jit(solution)/shard_map/dot_general | solution.py:17
  215.8 2.4 convolution_convert_fusion
  218.3 1.0 reshape.242
  219.2 3.3 %all-to-all-start.1 = ((bf16[32,4,2048]{2,1,0:T(4,128)(2,1)}), bf16[32,4,2048]{2,1,0:T(4,128)(2,1)S(1)}, u32[]{:S(2)}, u32[]{:S(2)}) async-start(bf16[32,4,2048]{2,1,0:T(4,128)(2,1)} %reshape.242), calls=%async_computation.1 | async-start | bytes 1048576 | tf_op jit(solution)/shard_map/all_to_all | solution.py:200
  222.6 14.2 %subtract_add_fusion = f32[24,16,4096]{2,1,0:T(8,128)} fusion(f32[24,16,4096]{2,1,0:T(8,128)} %mul.247, f32[24,16,4096]{2,1,0:T(8,128)} %mul.246, f32[24,16,4096]{2,1,0:T(8,128)} %param.35, f32[24,16,4096]{2,1,0:T(8,128)} %mul.244), kind=kLoop, calls=%fused_computation.5 | loop fusion | flops 4718592 | bytes 31457280 | tf_op jit(solution)/shard_map/add | solution.py:55
  236.8 2.0 fusion.74
  238.8 3.0 %fusion.9 = f32[24,2048]{1,0:T(8,128)S(1)} fusion(f32[24,2048]{1,0:T(8,128)S(1)} %get-tuple-element.13, bf16[512,2048]{1,0:T(8,128)(2,1)} %param.45, bf16[24,2048]{1,0:T(8,128)(2,1)S(1)} %copy-done.2, bf16[2048,512]{1,0:T(8,128)(2,1)} %param.44, f32[24,512]{1,0:T(8,128)S(1)} %fusion.74), kind=kOutput, calls=%fused_computation.16 | convolution fusion | flops 100884480 | bytes 4734976 | tf_op jit(solution)/shard_map/dot_general | solution.py:20
  241.8 1.3 fusion.7
  (76 shorter events, 12.4 us)
Async XLA Ops:
  7.2 208.7 %copy-start = (bf16[1,512,2048]{2,1,0:T(8,128)(2,1)S(1)}, bf16[1,512,2048]{2,1,0:T(8,128)(2,1)}, u32[]{:S(2)}) copy-start(bf16[1,512,2048]{2,1,0:T(8,128)(2,1)} %param.42) | copy-start | bytes 6291460
  7.2 66.1 %all-gather.3.cloned.1.call-start = ((), (), s32[]{:S(2)}) async-start(), calls=%async_computation.2 | async-start | bytes 3244032 | tf_op jit(solution)/shard_map/all_gather | solution.py:159
  81.6 14.8 %all-to-all-start = ((bf16[32,2,2304]{2,1,0:T(2,128)(2,1)}), bf16[32,2,2304]{2,1,0:T(2,128)(2,1)S(1)}, u32[]{:S(2)}, u32[]{:S(2)}) async-start(bf16[32,2,2304]{2,1,0:T(2,128)(2,1)} %reshape.259), calls=%async_computation | async-start | bytes 589824 | tf_op jit(solution)/shard_map/all_to_all | solution.py:163
  85.0 11.1 %copy-start.8 = (f32[1024]{0:T(1024)S(1)}, f32[1024]{0:T(1024)}, u32[]{:S(2)}) copy-start(f32[1024]{0:T(1024)} %param.31) | copy-start | bytes 12292
  85.0 11.2 %copy-start.9 = (f32[1024]{0:T(1024)S(1)}, f32[1024]{0:T(1024)}, u32[]{:S(2)}) copy-start(f32[1024]{0:T(1024)} %param.32) | copy-start | bytes 12292
  85.0 11.3 %copy-start.10 = (f32[1024]{0:T(1024)S(1)}, f32[1024]{0:T(1024)}, u32[]{:S(2)}) copy-start(f32[1024]{0:T(1024)} %param.33) | copy-start | bytes 12292
  85.0 11.3 %copy-start.11 = (f32[1024]{0:T(1024)S(1)}, f32[1024]{0:T(1024)}, u32[]{:S(2)}) copy-start(f32[1024]{0:T(1024)} %param.34) | copy-start | bytes 12292
  85.0 11.4 %copy-start.12 = (bf16[2048]{0:T(1024)(128)(2,1)S(1)}, bf16[2048]{0:T(1024)(128)(2,1)}, u32[]{:S(2)}) copy-start(bf16[2048]{0:T(1024)(128)(2,1)} %param.37) | copy-start | bytes 12292
  85.0 125.3 %all-gather.5.cloned.1.call-start = ((), (), s32[]{:S(2)}) async-start(), calls=%async_computation.3 | async-start | bytes 3244032 | tf_op jit(solution)/shard_map/all_gather | solution.py:188
  105.3 22.9 %copy-start.4 = (f32[24,16,64]{2,1,0:T(8,128)}, f32[24,16,64]{2,1,0:T(8,128)S(1)}, u32[]{:S(2)}) copy-start(f32[24,16,64]{2,1,0:T(8,128)S(1)} %fusion.41) | copy-start | bytes 294916
  105.5 22.8 %copy-start.1 = (f32[24,16,64,64]{3,2,1,0:T(8,128)S(1)}, f32[24,16,64,64]{3,2,1,0:T(8,128)}, u32[]{:S(2)}) copy-start(f32[24,16,64,64]{3,2,1,0:T(8,128)} %reshape.237) | copy-start | bytes 18874372
  105.5 22.8 %copy-start.6 = (bf16[24,16,64,1]{2,3,1,0:T(2,128)(2,1)S(1)}, bf16[24,16,64,1]{2,3,1,0:T(2,128)(2,1)}, u32[]{:S(2)}) copy-start(bf16[24,16,64,1]{2,3,1,0:T(2,128)(2,1)} %reshape.258) | copy-start | bytes 147460
  128.3 17.8 %copy-start.3 = (bf16[24,2048]{1,0:T(8,128)(2,1)S(1)}, bf16[24,2048]{1,0:T(8,128)(2,1)}, u32[]{:S(2)}) copy-start(bf16[24,2048]{1,0:T(8,128)(2,1)} %param.23) | copy-start | bytes 294916
  173.3 10.9 %copy-start.5 = (f32[24,16,64]{2,1,0:T(8,128)S(1)}, f32[24,16,64]{2,1,0:T(8,128)}, u32[]{:S(2)}) copy-start(f32[24,16,64]{2,1,0:T(8,128)} %copy-done.4) | copy-start | bytes 294916
  219.2 22.5 %all-to-all-start.1 = ((bf16[32,4,2048]{2,1,0:T(4,128)(2,1)}), bf16[32,4,2048]{2,1,0:T(4,128)(2,1)S(1)}, u32[]{:S(2)}, u32[]{:S(2)}) async-start(bf16[32,4,2048]{2,1,0:T(4,128)(2,1)} %reshape.242), calls=%async_computation.1 | async-start | bytes 1048576 | tf_op jit(solution)/shard_map/all_to_all | solution.py:200
  222.6 14.2 %copy-start.2 = (bf16[24,2048]{1,0:T(8,128)(2,1)S(1)}, bf16[24,2048]{1,0:T(8,128)(2,1)}, u32[]{:S(2)}) copy-start(bf16[24,2048]{1,0:T(8,128)(2,1)} %multiply_convert_fusion) | copy-start | bytes 294916
  236.8 5.0 %copy-start.7 = (f32[24,32]{1,0:T(8,128)S(1)}, f32[24,32]{1,0:T(8,128)}, u32[]{:S(2)}) copy-start(f32[24,32]{1,0:T(8,128)} %select_reduce_fusion) | copy-start | bytes 9220
Sparse Core Ops, SparseCore 0:
  11.4 61.7 all-gather.2
  150.0 60.2 all-gather.4
where the time goes:
time: 251 us; the launch traced here: 250 us
  local copies, waits for them, and re-layouts  70.5 us (28%)
  waiting for transfers between devices  66.8 us (27%)
  matrix products  59.4 us (24%)
  other arithmetic  32 us (13%)
  between operations  14.4 us (6%)
  starting transfers between devices  6.93 us (3%)
    all_gather x1, waiting for transfers between devices, per_device(): lax.all_gather(normed, 'ep', axis=0, tiled=True)  57 us
    dot_general x1, matrix products, attention_mixer(): jnp.einsum('nhvk,nhk->nhv', matrix, unit_key, precision=lax.Precision.HIG...  22.8 us
    dot_general x1, matrix products, attention_mixer(): jnp.einsum('nhvk,nhk->nhv', matrix, receptance_head, precision=lax.Precis...  16.5 us
    mul x2, local copies, waits for them, and re-layouts, attention_mixer(): matrix * heads(decay)[:, :, None, :]  16.3 us
    add x1, other arithmetic, attention_mixer(): matrix * heads(decay)[:, :, None, :]  14.2 us
    mul x1, local copies, waits for them, and re-layouts, attention_mixer(): recalled[..., None] * removal[:, :, None, :]  10.9 us
    reshape x1, local copies, waits for them, and re-layouts, attention_mixer(): matrix = head_state.reshape(tally_value, HEAD_COUNT, HEAD_SIZE, HEAD_SIZE)  10.8 us
    mul x1, local copies, waits for them, and re-layouts, attention_mixer(): head_value[..., None] * rate_scaled_key[:, :, None, :]  10.8 us
  transfers between devices with their start and end apart: 4, of which 2 were waited for; matrix products, arithmetic and copies ran while one was open for 35% of the time, Pallas kernels for 0%

commit v1 on v0

--- a/solution.py
+++ b/solution.py
@@ -6,6 +6,11 @@
 HEAD_COUNT = 16
 HEAD_SIZE = 64
 CAP = 4
+
+
+def swapped_in(array, mesh_axis, along):
+    sent = jnp.stack([array] * lax.axis_size(mesh_axis))
+    return jnp.concatenate(lax.all_to_all(sent, mesh_axis, 0, 0), axis=along)
 
 
 def rms_norm(value_rows, gain):
@@ -155,10 +160,7 @@
         axis=1,
     )
     local_cols = jnp.einsum(
-        "td,drc->trc",
-        lax.all_gather(normed, "ep", axis=0, tiled=True),
-        stacked,
-        preferred_element_type=jnp.float32,
+        "td,drc->trc", swapped_in(normed, "ep", 0), stacked, preferred_element_type=jnp.float32
     ).astype(jnp.bfloat16)
     role_rows = lax.all_to_all(local_cols, "ep", split_axis=0, concat_axis=2, tiled=True)
     normed_mixer_input, next_state = attention_mixer(

time: 251 us -> 270 us (1.076)
  waiting for transfers between devices: 66.8 us -> 77.1 us
  starting transfers between devices: 6.93 us -> 15 us
    all_to_all x0 -> x1, waiting for transfers between devices: none -> 67.3 us  [swapped_in(): return jnp.concatenate(lax.all_to_all(sent, mesh_axis, 0, 0), axis=along)]
    all_gather x1 -> x0, waiting for transfers between devices: 57 us -> none  [per_device(): lax.all_gather(normed, 'ep', axis=0, tiled=True)]
    all_to_all x0 -> x1, starting transfers between devices: none -> 7.45 us  [swapped_in(): return jnp.concatenate(lax.all_to_all(sent, mesh_axis, 0, 0), axis=along)]
    unnamed x33 -> x45, local copies, waits for them, and re-layouts: 10.3 us -> 9.05 us
  transfers between devices with their start and end apart: 4 -> 4, of which waited for: 2 -> 2; matrix products, arithmetic and copies ran while one was open for 35% -> 32% of each run, Pallas kernels for 0% -> 0%
where the time goes in v1:
time: 270 us; the launch traced here: 269 us
  waiting for transfers between devices  77.1 us (29%)
  local copies, waits for them, and re-layouts  71 us (26%)
  matrix products  59.6 us (22%)
  other arithmetic  31.3 us (12%)
  starting transfers between devices  15 us (6%)
  between operations  14.4 us (5%)
    all_to_all x1, waiting for transfers between devices, swapped_in(): return jnp.concatenate(lax.all_to_all(sent, mesh_axis, 0, 0), axis=along)  67.3 us
    dot_general x1, matrix products, attention_mixer(): jnp.einsum('nhvk,nhk->nhv', matrix, unit_key, precision=lax.Precision.HIG...  22.8 us
    dot_general x1, matrix products, attention_mixer(): jnp.einsum('nhvk,nhk->nhv', matrix, receptance_head, precision=lax.Precis...  16.5 us
    mul x2, local copies, waits for them, and re-layouts, attention_mixer(): matrix * heads(decay)[:, :, None, :]  16.3 us
    add x1, other arithmetic, attention_mixer(): matrix * heads(decay)[:, :, None, :]  14.2 us
    mul x1, local copies, waits for them, and re-layouts, attention_mixer(): recalled[..., None] * removal[:, :, None, :]  10.9 us
    reshape x1, local copies, waits for them, and re-layouts, attention_mixer(): matrix = head_state.reshape(tally_value, HEAD_COUNT, HEAD_SIZE, HEAD_SIZE)  10.9 us
    mul x1, local copies, waits for them, and re-layouts, attention_mixer(): head_value[..., None] * rate_scaled_key[:, :, None, :]  10.8 us
  transfers between devices with their start and end apart: 4, of which 2 were waited for; matrix products, arithmetic and copies ran while one was open for 32% of the time, Pallas kernels for 0%

profile of v1, /device:TPU:0, one launch (start us, length us, event | category | flops | bytes accessed | tf_op | source)
XLA Modules:
  0.0 268.5 jit_solution(2481296854341186128)
XLA Ops:
  8.0 1.0 fusion.34
  9.0 1.0 fusion.36
  10.1 2.1 stack.16
  12.1 7.4 %all-to-all-start = ((bf16[32,24,2048]{2,1,0:T(8,128)(2,1)}), bf16[32,24,2048]{2,1,0:T(8,128)(2,1)}, u32[]{:S(2)}, u32[]{:S(2)}) async-start(bf16[32,24,2048]{2,1,0:T(8,128)(2,1)} %stack.16), calls=%async_computation | async-start | bytes 6291456 | tf_op jit(solution)/shard_map/all_to_all | solution.py:13
  23.6 67.3 %all-to-all-done = bf16[32,24,2048]{2,1,0:T(8,128)(2,1)} async-done(((bf16[32,24,2048]{2,1,0:T(8,128)(2,1)}), bf16[32,24,2048]{2,1,0:T(8,128)(2,1)}, u32[]{:S(2)}, u32[]{:S(2)}) %all-to-all-start) | async-done | bytes 3145760 | tf_op jit(solution)/shard_map/all_to_all | solution.py:13
  90.9 3.3 %fusion.72 = f32[768,192]{0,1:S(1)} fusion(bf16[768,2048]{1,0:T(8,128)(2,1)} %bitcast, bf16[2048,192]{0,1:T(8,128)(2,1)} %bitcast.7), kind=kOutput, calls=%fused_computation.110 | convolution fusion | flops 603979776 | bytes 4521984
  94.2 1.8 copy.38
  96.0 3.4 %reshape.265 = bf16[32,2,2304]{2,1,0:T(2,128)(2,1)} reshape(bf16[768,6,32]{2,1,0:T(8,128)(2,1)} %copy.38) | data formatting | bytes 589824
  99.5 4.0 %all-to-all-start.1 = ((bf16[32,2,2304]{2,1,0:T(2,128)(2,1)}), bf16[32,2,2304]{2,1,0:T(2,128)(2,1)S(1)}, u32[]{:S(2)}, u32[]{:S(2)}) async-start(bf16[32,2,2304]{2,1,0:T(2,128)(2,1)} %reshape.265), calls=%async_computation.1 | async-start | bytes 589824 | tf_op jit(solution)/shard_map/all_to_all | solution.py:165
  103.8 10.9 %reshape.242 = f32[24,16,64,64]{3,2,1,0:T(8,128)} reshape(f32[24,16,4096]{2,1,0:T(8,128)} %param.35) | data formatting | bytes 12582912 | tf_op jit(solution)/shard_map/reshape | solution.py:57
  115.0 2.2 reshape.266
  117.2 2.2 copy.40
  119.3 1.9 all_to_all.23
  121.3 0.9 slice_convert_fusion.2
  124.0 22.8 %fusion.73 = f32[24,16,1,64]{3,2,1,0:T(1,128)S(1)} fusion(f32[24,16,64,1]{2,3,1,0:T(1,128)S(1)} %bitcast.98, f32[24,16,64,64]{3,2,1,0:T(8,128)} %reshape.242), kind=kOutput, calls=%fused_computation.111 | convolution fusion | flops 18874368 | bytes 6488064 | tf_op jit(solution)/shard_map/nhvk,nhk->nhv/dot_general | solution.py:58
  146.9 16.5 %fusion.1 = f32[24,16,1,64]{3,2,1,0:T(1,128)S(1)} fusion(bf16[24,16,64,1]{2,3,1,0:T(2,128)(2,1)S(1)} %copy-done.6, f32[24,16,64,64]{3,2,1,0:T(8,128)S(1)} %copy-done.1, f32[24,16,64]{2,1,0:T(8,128)S(1)} %fusion.41, f32[24,16,64]{2,1,0:T(8,128)S(1)} %get-tuple-element.2, f32[24,16,64]{2,1,0:T(8,128)S(1)} %bitcast.96, f32[24,16,64]{2,1,0:T(8,128)S(1)} %get-tuple-element.4, ...), kind=kOutput, calls=%fused_computation.1 | convolution fusion | flops 26738688 | bytes 6930432 | tf_op jit(solution)/shard_map/nhvk,nhk->nhv/dot_general | solution.py:64
  164.7 3.0 %multiply_reduce_fusion = (f32[24]{0:T(128)S(1)}, f32[24,2048]{1,0:T(8,128)S(1)}) fusion(bf16[1024,2048]{1,0:T(8,128)(2,1)} %param.36, f32[24,1024]{1,0:T(8,128)S(1)} %reshape.245, bf16[24,6,1024]{2,0,1:T(8,128)(2,1)} %all_to_all.23, bf16[24,2048]{1,0:T(8,128)(2,1)S(1)} %copy-done.3), kind=kOutput, calls=%fused_computation.49 | convolution fusion | flops 101105640 | bytes 4636768 | tf_op jit(solution)/shard_map/dot_general | solution.py:179
  171.8 9.3 %broadcast_multiply_fusion = (f32[24,16,64,64]{3,2,1,0:T(8,128)}, f32[24,16,64,64]{3,2,1,0:T(8,128)}) fusion(f32[24,16,64]{2,1,0:T(8,128)S(1)} %get-tuple-element.4, f32[24,16,64]{2,1,0:T(8,128)S(1)} %reshape.252, f32[24,16,64]{2,1,0:T(8,128)S(1)} %get-tuple-element.2, f32[24,16,64]{2,1,0:T(8,128)S(1)} %bitcast.97), kind=kLoop, calls=%fused_computation.6 | loop fusion | flops 3145728 | bytes 12976128 | tf_op jit(solution)/shard_map/mul | solution.py:62
  181.1 10.8 %mul.247 = f32[24,16,4096]{2,1,0:T(8,128)} reshape(f32[24,16,64,64]{3,2,1,0:T(8,128)} %get-tuple-element.14) | data formatting | bytes 12582912 | tf_op jit(solution)/shard_map/mul | solution.py:62
  191.9 10.9 %mul.246 = f32[24,16,4096]{2,1,0:T(8,128)} reshape(f32[24,16,64,64]{3,2,1,0:T(8,128)} %get-tuple-element.15) | data formatting | bytes 12582912 | tf_op jit(solution)/shard_map/mul | solution.py:61
  202.8 5.4 %mul.206 = f32[24,16,64,64]{3,2,1,0:T(8,128)} broadcast(f32[24,16,64]{2,1,0:T(8,128)S(1)} %copy-done.5), dimensions={0,1,3} | broadcast | bytes 6389760 | tf_op jit(solution)/shard_map/mul | solution.py:60
  208.2 10.9 %mul.244 = f32[24,16,4096]{2,1,0:T(8,128)} reshape(f32[24,16,64,64]{3,2,1,0:T(8,128)} %mul.206) | data formatting | bytes 12582912 | tf_op jit(solution)/shard_map/mul | solution.py:60
  219.1 9.8 %all-gather.2.cloned.1.call-done = bf16[768,2048]{1,0:T(8,128)(2,1)} async-done(((bf16[24,2048]{1,0:T(8,128)(2,1)}), bf16[768,2048]{1,0:T(8,128)(2,1)}) %all-gather.2.cloned.1.call-update) | async-done | bytes 3145744 | tf_op jit(solution)/shard_map/all_gather | solution.py:190
  228.9 2.7 convolution_convert_fusion.1
  231.7 2.7 %fusion.15 = f32[128,512]{1,0:T(8,128)} fusion(bf16[128,2048]{1,0:T(8,128)(2,1)S(1)} %reshape.247, bf16[1,2048,512]{2,1,0:T(8,128)(2,1)} %param.40), kind=kOutput, calls=%fused_computation.23 | convolution fusion | flops 268435456 | bytes 2883584 | tf_op jit(solution)/shard_map/dot_general | solution.py:22
  234.4 2.4 convolution_convert_fusion
  236.9 1.0 reshape.248
  237.8 3.3 %all-to-all-start.2 = ((bf16[32,4,2048]{2,1,0:T(4,128)(2,1)}), bf16[32,4,2048]{2,1,0:T(4,128)(2,1)S(1)}, u32[]{:S(2)}, u32[]{:S(2)}) async-start(bf16[32,4,2048]{2,1,0:T(4,128)(2,1)} %reshape.248), calls=%async_computation.2 | async-start | bytes 1048576 | tf_op jit(solution)/shard_map/all_to_all | solution.py:202
  241.2 14.2 %subtract_add_fusion = f32[24,16,4096]{2,1,0:T(8,128)} fusion(f32[24,16,4096]{2,1,0:T(8,128)} %mul.247, f32[24,16,4096]{2,1,0:T(8,128)} %mul.246, f32[24,16,4096]{2,1,0:T(8,128)} %param.35, f32[24,16,4096]{2,1,0:T(8,128)} %mul.244), kind=kLoop, calls=%fused_computation.5 | loop fusion | flops 4718592 | bytes 31457280 | tf_op jit(solution)/shard_map/add | solution.py:60
  255.4 2.0 fusion.74
  257.4 3.0 %fusion.9 = f32[24,2048]{1,0:T(8,128)S(1)} fusion(f32[24,2048]{1,0:T(8,128)S(1)} %get-tuple-element.13, bf16[512,2048]{1,0:T(8,128)(2,1)} %param.45, bf16[24,2048]{1,0:T(8,128)(2,1)S(1)} %copy-done.2, bf16[2048,512]{1,0:T(8,128)(2,1)} %param.44, f32[24,512]{1,0:T(8,128)S(1)} %fusion.74), kind=kOutput, calls=%fused_computation.16 | convolution fusion | flops 100884480 | bytes 4734976 | tf_op jit(solution)/shard_map/dot_general | solution.py:25
  260.4 1.3 fusion.7
  (88 shorter events, 12.7 us)
Async XLA Ops:
  7.2 227.3 %copy-start = (bf16[1,512,2048]{2,1,0:T(8,128)(2,1)S(1)}, bf16[1,512,2048]{2,1,0:T(8,128)(2,1)}, u32[]{:S(2)}) copy-start(bf16[1,512,2048]{2,1,0:T(8,128)(2,1)} %param.42) | copy-start | bytes 6291460
  10.0 9.5 %copy-start.7 = (bf16[2048,32]{0,1:T(8,128)(2,1)S(1)}, bf16[2048,32]{0,1:T(8,128)(2,1)}, u32[]{:S(2)}) copy-start(bf16[2048,32]{0,1:T(8,128)(2,1)} %param.25) | copy-start | bytes 393220
  10.1 10.2 %copy-start.8 = (bf16[2048,32]{0,1:T(8,128)(2,1)S(1)}, bf16[2048,32]{0,1:T(8,128)(2,1)}, u32[]{:S(2)}) copy-start(bf16[2048,32]{0,1:T(8,128)(2,1)} %param.26) | copy-start | bytes 393220
  12.1 8.8 %copy-start.9 = (bf16[2048,32]{0,1:T(8,128)(2,1)S(1)}, bf16[2048,32]{0,1:T(8,128)(2,1)}, u32[]{:S(2)}) copy-start(bf16[2048,32]{0,1:T(8,128)(2,1)} %param.27) | copy-start | bytes 393220
  12.1 9.5 %copy-start.10 = (bf16[2048,32]{0,1:T(8,128)(2,1)S(1)}, bf16[2048,32]{0,1:T(8,128)(2,1)}, u32[]{:S(2)}) copy-start(bf16[2048,32]{0,1:T(8,128)(2,1)} %param.28) | copy-start | bytes 393220
  12.1 10.1 %copy-start.11 = (bf16[2048,32]{0,1:T(8,128)(2,1)S(1)}, bf16[2048,32]{0,1:T(8,128)(2,1)}, u32[]{:S(2)}) copy-start(bf16[2048,32]{0,1:T(8,128)(2,1)} %param.29) | copy-start | bytes 393220
  12.1 10.8 %copy-start.12 = (bf16[2048,32]{0,1:T(8,128)(2,1)S(1)}, bf16[2048,32]{0,1:T(8,128)(2,1)}, u32[]{:S(2)}) copy-start(bf16[2048,32]{0,1:T(8,128)(2,1)} %param.30) | copy-start | bytes 393220
  12.1 78.8 %all-to-all-start = ((bf16[32,24,2048]{2,1,0:T(8,128)(2,1)}), bf16[32,24,2048]{2,1,0:T(8,128)(2,1)}, u32[]{:S(2)}, u32[]{:S(2)}) async-start(bf16[32,24,2048]{2,1,0:T(8,128)(2,1)} %stack.16), calls=%async_computation | async-start | bytes 6291456 | tf_op jit(solution)/shard_map/all_to_all | solution.py:13
  99.5 15.5 %all-to-all-start.1 = ((bf16[32,2,2304]{2,1,0:T(2,128)(2,1)}), bf16[32,2,2304]{2,1,0:T(2,128)(2,1)S(1)}, u32[]{:S(2)}, u32[]{:S(2)}) async-start(bf16[32,2,2304]{2,1,0:T(2,128)(2,1)} %reshape.265), calls=%async_computation.1 | async-start | bytes 589824 | tf_op jit(solution)/shard_map/all_to_all | solution.py:165
  103.5 11.1 %copy-start.14 = (f32[1024]{0:T(1024)S(1)}, f32[1024]{0:T(1024)}, u32[]{:S(2)}) copy-start(f32[1024]{0:T(1024)} %param.31) | copy-start | bytes 12292
  103.5 11.2 %copy-start.15 = (f32[1024]{0:T(1024)S(1)}, f32[1024]{0:T(1024)}, u32[]{:S(2)}) copy-start(f32[1024]{0:T(1024)} %param.32) | copy-start | bytes 12292
  103.6 11.3 %copy-start.16 = (f32[1024]{0:T(1024)S(1)}, f32[1024]{0:T(1024)}, u32[]{:S(2)}) copy-start(f32[1024]{0:T(1024)} %param.33) | copy-start | bytes 12292
  103.6 11.3 %copy-start.17 = (f32[1024]{0:T(1024)S(1)}, f32[1024]{0:T(1024)}, u32[]{:S(2)}) copy-start(f32[1024]{0:T(1024)} %param.34) | copy-start | bytes 12292
  103.6 11.4 %copy-start.18 = (bf16[2048]{0:T(1024)(128)(2,1)S(1)}, bf16[2048]{0:T(1024)(128)(2,1)}, u32[]{:S(2)}) copy-start(bf16[2048]{0:T(1024)(128)(2,1)} %param.37) | copy-start | bytes 12292
  103.6 125.3 %all-gather.2.cloned.1.call-start = ((), (), s32[]{:S(2)}) async-start(), calls=%async_computation.3 | async-start | bytes 3244032 | tf_op jit(solution)/shard_map/all_gather | solution.py:190
  123.9 23.0 %copy-start.4 = (f32[24,16,64]{2,1,0:T(8,128)}, f32[24,16,64]{2,1,0:T(8,128)S(1)}, u32[]{:S(2)}) copy-start(f32[24,16,64]{2,1,0:T(8,128)S(1)} %fusion.41) | copy-start | bytes 294916
  124.0 22.8 %copy-start.1 = (f32[24,16,64,64]{3,2,1,0:T(8,128)S(1)}, f32[24,16,64,64]{3,2,1,0:T(8,128)}, u32[]{:S(2)}) copy-start(f32[24,16,64,64]{3,2,1,0:T(8,128)} %reshape.242) | copy-start | bytes 18874372
  124.0 22.8 %copy-start.6 = (bf16[24,16,64,1]{2,3,1,0:T(2,128)(2,1)S(1)}, bf16[24,16,64,1]{2,3,1,0:T(2,128)(2,1)}, u32[]{:S(2)}) copy-start(bf16[24,16,64,1]{2,3,1,0:T(2,128)(2,1)} %reshape.264) | copy-start | bytes 147460
  146.9 17.8 %copy-start.3 = (bf16[24,2048]{1,0:T(8,128)(2,1)S(1)}, bf16[24,2048]{1,0:T(8,128)(2,1)}, u32[]{:S(2)}) copy-start(bf16[24,2048]{1,0:T(8,128)(2,1)} %param.23) | copy-start | bytes 294916
  191.9 10.9 %copy-start.5 = (f32[24,16,64]{2,1,0:T(8,128)S(1)}, f32[24,16,64]{2,1,0:T(8,128)}, u32[]{:S(2)}) copy-start(f32[24,16,64]{2,1,0:T(8,128)} %copy-done.4) | copy-start | bytes 294916
  237.8 22.5 %all-to-all-start.2 = ((bf16[32,4,2048]{2,1,0:T(4,128)(2,1)}), bf16[32,4,2048]{2,1,0:T(4,128)(2,1)S(1)}, u32[]{:S(2)}, u32[]{:S(2)}) async-start(bf16[32,4,2048]{2,1,0:T(4,128)(2,1)} %reshape.248), calls=%async_computation.2 | async-start | bytes 1048576 | tf_op jit(solution)/shard_map/all_to_all | solution.py:202
  241.2 14.2 %copy-start.2 = (bf16[24,2048]{1,0:T(8,128)(2,1)S(1)}, bf16[24,2048]{1,0:T(8,128)(2,1)}, u32[]{:S(2)}) copy-start(bf16[24,2048]{1,0:T(8,128)(2,1)} %multiply_convert_fusion) | copy-start | bytes 294916
  255.4 5.0 %copy-start.13 = (f32[24,32]{1,0:T(8,128)S(1)}, f32[24,32]{1,0:T(8,128)}, u32[]{:S(2)}) copy-start(f32[24,32]{1,0:T(8,128)} %select_reduce_fusion) | copy-start | bytes 9220
Sparse Core Ops, SparseCore 0:
  168.6 60.2 all-gather.1
